TPU v7x, 32 devices: a whole 2x2x4 slice. The times are simulated.
32 devices in a mesh: grp: 2 (over y), sp: 4 (over z), tp: 4 (over x, core).
Axes of the slice: x: 2, y: 2, z: 4, core: 2. Of those that a mesh axis runs over, the one named last changes fastest.
Arguments:
- latent: bfloat16 [2048, 512], P(('grp', 'sp')), parts along dimension 0, may hold values from -6 to 6
- rope_key: bfloat16 [2048, 64], P(('grp', 'sp')), parts along dimension 0, may hold values from -6 to 6
- wide_query: bfloat16 [2048, 1536], P(('grp', 'sp'), 'tp'), parts along dimension 0, may hold values from -1300 to 1300
- narrow_query: bfloat16 [2048, 1024], P(('grp', 'sp'), 'tp'), parts along dimension 0, may hold values from -1300 to 1300
- wide_key_weight: bfloat16 [512, 1024], P(None, 'tp'), may hold values from -0.25 to 0.25
- wide_value_weight: bfloat16 [512, 1024], P(None, 'tp'), may hold values from -0.25 to 0.25
- narrow_key_weight: bfloat16 [512, 512], P(None, 'tp'), may hold values from -0.25 to 0.25
- narrow_value_weight: bfloat16 [512, 512], P(None, 'tp'), may hold values from -0.25 to 0.25
- latent_norm_scale: float32 [512], replicated, may hold values from 0.1 to 1.9
- out_wide: bfloat16 [1024, 4096], P('tp'), may hold values from -0.4375 to 0.4375
- out_narrow: bfloat16 [512, 4096], P('tp'), may hold values from -0.4375 to 0.4375
- residual: bfloat16 [2048, 4096], P(('grp', 'sp', 'tp')), parts along dimension 0, may hold values from -6 to 6
- ffn_gain: float32 [4096], replicated, may hold values from 0.1 to 1.9
- shared_gate: bfloat16 [4096, 512], P(None, 'tp'), may hold values from -0.09375 to 0.09375
- shared_up: bfloat16 [4096, 512], P(None, 'tp'), may hold values from -0.09375 to 0.09375
- shared_down: bfloat16 [512, 4096], P('tp'), may hold values from -0.25 to 0.25
- expert_gate: bfloat16 [16, 4096, 192], P(('sp', 'tp')), may hold values from -0.09375 to 0.09375
- expert_up: bfloat16 [16, 4096, 192], P(('sp', 'tp')), may hold values from -0.09375 to 0.09375
- expert_down: bfloat16 [16, 192, 4096], P(('sp', 'tp')), may hold values from -0.4375 to 0.4375
- routes: int32 [2048, 2], P(('grp', 'sp', 'tp')), parts along dimension 0, may hold values from 0 to 15, all different within a row; in each aligned block of 64 rows (0 to 63, 64 to 127, ...) at most 16 rows name the same one
- route_weights: float32 [2048, 2], P(('grp', 'sp', 'tp')), parts along dimension 0, may hold values from 0.25 to 1.5
Outputs:
- layer_out: bfloat16 [2048, 4096], P(('grp', 'sp', 'tp')), parts along dimension 0
There are 2 independent parts, one for each index of `grp`. A program takes and returns all parts, laid end to end along the dimension named above; an argument that names none is the same for every part. Nothing has to cross between parts.
Inputs may be any that keep to these rules, and one draw needn't show every extreme that they name: `routes`: each row names 2 different experts; in each aligned block of 64 rows no expert is named by more than 16 rows, and some block has an expert named exactly 16 times.
All inputs are finite; a program needn't handle non-finite values.
Results may differ from a plain program's by a relative error of at most 0.023.
Values may be sent and summed in bfloat16 or wider, within the bound.
A program may use at most 128 MiB of HBM per device.

v0:
```python
import math

import jax
import jax.numpy as jnp
from jax import lax
from jax.sharding import PartitionSpec as P

ROPE = 64
WIDE_HEAD_SIZE = 128
NARROW_HEAD_SIZE = 64


EPS = 1e-06
ROPE_BASE = 10000.0
NEG_FILL = -1e30


def rotate(values, positions):
    half_size = values.shape[-1] // 2
    inverse = ROPE_BASE ** (-jnp.arange(half_size, dtype=jnp.float32) * 2.0 / values.shape[-1])
    angles = positions.astype(jnp.float32)[:, None] * inverse[None, :]
    shaped = (angles.shape[0],) + (1,) * (values.ndim - 2) + (half_size,)
    cosine_table = jnp.cos(angles).reshape(shaped)
    sine_table = jnp.sin(angles).reshape(shaped)
    first_half = values[..., :half_size]
    second_half = values[..., half_size:]
    return jnp.concatenate(
        [
            first_half * cosine_table - second_half * sine_table,
            second_half * cosine_table + first_half * sine_table,
        ],
        axis=-1,
    )


def rms_scale(values, gain):
    return values * lax.rsqrt(jnp.mean(values * values, axis=-1, keepdims=True) + EPS) * gain


def update(state, query_plain, query_turned, keys, turned_rows, values, visible, factor):
    running_max, running_sum, weighted = state
    scores = jnp.einsum("qhd,khd->hqk", query_plain, keys, preferred_element_type=jnp.float32)
    scores = scores + jnp.einsum(
        "qhr,kr->hqk", query_turned, turned_rows, preferred_element_type=jnp.float32
    )
    scores = jnp.where(visible[None], scores * factor, NEG_FILL)
    new_max = jnp.maximum(running_max, jnp.max(scores, axis=2))
    probs = jnp.where(visible[None], jnp.exp(scores - new_max[:, :, None]), 0.0)
    fading = jnp.exp(running_max - new_max)
    running_sum = running_sum * fading + jnp.sum(probs, axis=2)
    weighted = weighted * fading[:, :, None] + jnp.einsum(
        "hqk,khd->hqd", probs.astype(jnp.bfloat16), values, preferred_element_type=jnp.float32
    )
    return (new_max, running_sum, weighted)


def empty_state(heads, queries, value_size):
    return (
        jnp.full((heads, queries), NEG_FILL, jnp.float32),
        jnp.zeros((heads, queries), jnp.float32),
        jnp.zeros((heads, queries, value_size), jnp.float32),
    )


def finish(state):
    normal_sampler = state[2] / state[1][:, :, None]
    heads, queries, value_size = normal_sampler.shape
    return (
        normal_sampler.astype(jnp.bfloat16).transpose(1, 0, 2).reshape(queries, heads * value_size)
    )


def body(
    latent,
    rope_key,
    wide_query,
    narrow_query,
    wide_key_weight,
    wide_value_weight,
    narrow_key_weight,
    narrow_value_weight,
    latent_norm_scale,
    out_wide,
    out_narrow,
    residual,
    ffn_gain,
    shared_gate,
    shared_up,
    shared_down,
    expert_gate,
    expert_up,
    expert_down,
    routes,
    route_weights,
):
    tok_dev = latent.shape[0]
    seq_index = lax.axis_index("sp")
    own_pos = seq_index * tok_dev + jnp.arange(tok_dev, dtype=jnp.int32)
    last_pos = seq_index * tok_dev + tok_dev - 1
    normed_latent = rms_scale(latent.astype(jnp.float32), latent_norm_scale).astype(jnp.bfloat16)
    turned_key = rotate(rope_key.astype(jnp.float32), own_pos).astype(jnp.bfloat16)
    wide_heads_q = wide_query.reshape(tok_dev, -1, WIDE_HEAD_SIZE + ROPE)
    wide_plain = wide_heads_q[..., :WIDE_HEAD_SIZE]
    wide_turned = rotate(wide_heads_q[..., WIDE_HEAD_SIZE:].astype(jnp.float32), own_pos).astype(
        jnp.bfloat16
    )
    narrow_heads_q = narrow_query.reshape(tok_dev, -1, NARROW_HEAD_SIZE + ROPE)
    narrow_plain = narrow_heads_q[..., :NARROW_HEAD_SIZE]
    narrow_turned = rotate(
        narrow_heads_q[..., NARROW_HEAD_SIZE:].astype(jnp.float32), own_pos
    ).astype(jnp.bfloat16)
    wide_local = wide_plain.shape[1]
    narrow_local = narrow_plain.shape[1]
    wide_factor = (WIDE_HEAD_SIZE + ROPE) ** (-0.5)
    narrow_factor = (NARROW_HEAD_SIZE + ROPE) ** (-0.5)
    initial = empty_state(wide_local, tok_dev, WIDE_HEAD_SIZE) + empty_state(
        narrow_local, tok_dev, NARROW_HEAD_SIZE
    )
    pieces = (
        lax.all_gather(normed_latent, "sp", axis=0, tiled=True),
        lax.all_gather(turned_key, "sp", axis=0, tiled=True),
    )
    indices = jnp.arange(pieces[0].shape[0], dtype=jnp.int32)
    placing = lambda positions: positions
    latent_rows, turned_rows = pieces
    length_rows = latent_rows.shape[0]
    block = math.gcd(length_rows, 512)

    def one_block(block_index, inner):
        lat_block = lax.dynamic_slice_in_dim(latent_rows, block_index * block, block, 0)
        turned_block = lax.dynamic_slice_in_dim(turned_rows, block_index * block, block, 0)
        key_pos = placing(lax.dynamic_slice_in_dim(indices, block_index * block, block, 0))

        def work(current):
            visible = key_pos[None, :] <= own_pos[:, None]
            wide_keys = (
                jnp.dot(lat_block, wide_key_weight, preferred_element_type=jnp.float32)
                .astype(jnp.bfloat16)
                .reshape(block, wide_local, WIDE_HEAD_SIZE)
            )
            wide_values = (
                jnp.dot(lat_block, wide_value_weight, preferred_element_type=jnp.float32)
                .astype(jnp.bfloat16)
                .reshape(block, wide_local, WIDE_HEAD_SIZE)
            )
            narrow_keys = (
                jnp.dot(lat_block, narrow_key_weight, preferred_element_type=jnp.float32)
                .astype(jnp.bfloat16)
                .reshape(block, narrow_local, NARROW_HEAD_SIZE)
            )
            narrow_values = (
                jnp.dot(lat_block, narrow_value_weight, preferred_element_type=jnp.float32)
                .astype(jnp.bfloat16)
                .reshape(block, narrow_local, NARROW_HEAD_SIZE)
            )
            wide_state = update(
                current[:3],
                wide_plain,
                wide_turned,
                wide_keys,
                turned_block,
                wide_values,
                visible,
                wide_factor,
            )
            narrow_state = update(
                current[3:],
                narrow_plain,
                narrow_turned,
                narrow_keys,
                turned_block,
                narrow_values,
                visible,
                narrow_factor,
            )
            return wide_state + narrow_state

        return lax.cond(jnp.min(key_pos) <= last_pos, work, lambda current: current, inner)

    final = lax.fori_loop(0, length_rows // block, one_block, initial)
    wide_mix = finish(final[:3])
    narrow_mix = finish(final[3:])
    projected = lax.psum_scatter(
        (
            jnp.dot(wide_mix, out_wide, preferred_element_type=jnp.float32)
            + jnp.dot(narrow_mix, out_narrow, preferred_element_type=jnp.float32)
        ).astype(jnp.bfloat16),
        "tp",
        scatter_dimension=0,
        tiled=True,
    ).astype(jnp.float32)
    stream = (residual.astype(jnp.float32) + projected).astype(jnp.bfloat16)
    normed = rms_scale(stream.astype(jnp.float32), ffn_gain).astype(jnp.bfloat16)
    piece = lax.all_gather(normed, "tp", axis=0, tiled=True)
    gate_part = jnp.dot(piece, shared_gate, preferred_element_type=jnp.float32)
    up_part = jnp.dot(piece, shared_up, preferred_element_type=jnp.float32)
    active = (jax.nn.silu(gate_part) * up_part).astype(jnp.bfloat16)
    shared_terms = jnp.dot(active, shared_down, preferred_element_type=jnp.float32)
    shared = lax.psum_scatter(
        shared_terms.astype(jnp.bfloat16), "tp", scatter_dimension=0, tiled=True
    ).astype(jnp.float32)
    rows_here, top_count = routes.shape
    local_experts = expert_gate.shape[0]
    experts_all = local_experts * lax.axis_size(("sp", "tp"))
    capacity = max(2, 2 * top_count * rows_here // experts_all)
    model_width = normed.shape[1]
    flat_routes = routes.reshape(-1)
    assigned = flat_routes.shape[0]
    choose = (flat_routes[:, None] == jnp.arange(experts_all, dtype=jnp.int32)[None, :]).astype(
        jnp.float32
    )
    lower_mask = (jnp.arange(assigned)[:, None] > jnp.arange(assigned)[None, :]).astype(jnp.float32)
    earlier = jnp.dot(lower_mask, choose, precision=lax.Precision.HIGHEST)
    slots = jnp.sum(earlier * choose, axis=1).astype(jnp.int32)
    target = flat_routes * capacity + slots
    send_map = jnp.any(
        target.reshape(rows_here, top_count)[None, :, :]
        == jnp.arange(experts_all * capacity, dtype=jnp.int32)[:, None, None],
        axis=2,
    ).astype(jnp.bfloat16)
    outgoing = jnp.dot(send_map, normed, preferred_element_type=jnp.float32).astype(jnp.bfloat16)
    outgoing = outgoing.reshape(experts_all, capacity, model_width)
    incoming = lax.all_to_all(outgoing, ("sp", "tp"), split_axis=0, concat_axis=0, tiled=True)
    sources = incoming.shape[0] // local_experts
    grouped = incoming.reshape(sources, local_experts, incoming.shape[1], model_width)
    gate_part = jnp.einsum(
        "sxcd,xdf->sxcf", grouped, expert_gate, preferred_element_type=jnp.float32
    )
    up_part = jnp.einsum("sxcd,xdf->sxcf", grouped, expert_up, preferred_element_type=jnp.float32)
    active = (jax.nn.silu(gate_part) * up_part).astype(jnp.bfloat16)
    finished = jnp.einsum(
        "sxcf,xfd->sxcd", active, expert_down, preferred_element_type=jnp.float32
    ).astype(jnp.bfloat16)
    returned = lax.all_to_all(
        finished.reshape(incoming.shape), ("sp", "tp"), split_axis=0, concat_axis=0, tiled=True
    )
    picked = returned.reshape(experts_all * capacity, model_width)[target]
    routed = jnp.sum(
        picked.reshape(rows_here, top_count, model_width).astype(jnp.float32)
        * route_weights[:, :, None],
        axis=1,
    )
    return (stream.astype(jnp.float32) + shared + routed).astype(jnp.bfloat16)


def solution(mesh):
    placed = (
        P(("grp", "sp"), None),
        P(("grp", "sp"), None),
        P(("grp", "sp"), "tp"),
        P(("grp", "sp"), "tp"),
        P(None, "tp"),
        P(None, "tp"),
        P(None, "tp"),
        P(None, "tp"),
        P(),
        P("tp", None),
        P("tp", None),
        P(("grp", "sp", "tp"), None),
        P(),
        P(None, "tp"),
        P(None, "tp"),
        P("tp", None),
        P(("sp", "tp"), None, None),
        P(("sp", "tp"), None, None),
        P(("sp", "tp"), None, None),
        P(("grp", "sp", "tp"), None),
        P(("grp", "sp", "tp"), None),
    )
    return jax.shard_map(
        body, mesh=mesh, in_specs=placed, out_specs=P(("grp", "sp", "tp"), None), check_vma=False
    )
```

profile of v0, /device:TPU:27, one launch (start us, length us, event | category | flops | bytes accessed | tf_op | source)
XLA Modules:
  0.0 234.9 jit_solution(14494087974197204118)
XLA Ops:
  6.5 1.2 fusion.66
  7.8 1.8 fusion.68
  10.5 1.7 copy.48
  13.6 11.6 %all_gather.10 = bf16[1024,64]{0,1:T(8,128)(2,1)S(1)} all-gather(bf16[256,64]{0,1:T(8,128)(2,1)S(1)} %pad_maximum_fusion.2), channel_id=1, replica_groups=mesh['grp'=2,'sp'=4,'tp'=4] {'sp'}, dimensions={0}, use_global_device_ids=true | all-gather | bytes 163840 | tf_op jit(solution)/shard_map/all_gather | solution.py:121
  25.2 1.5 slice_convert_fusion
  27.4 11.3 %all-gather.3.cloned.1.call-done = bf16[1024,512]{1,0:T(8,128)(2,1)} async-done(((bf16[256,512]{1,0:T(8,128)(2,1)}), bf16[1024,512]{1,0:T(8,128)(2,1)}) %all-gather.3.cloned.1.call-update) | async-done | bytes 1048592 | tf_op jit(solution)/shard_map/all_gather | solution.py:120
  40.0 16.7 %while.24 = (s32[]{:T(128)}, f32[2,256]{1,0:T(2,128)S(1)}, f32[2,256]{1,0:T(2,128)S(1)}, f32[2,256,128]{2,1,0:T(8,128)S(1)}, f32[2,256]{1,0:T(2,128)S(1)}, /*ind...) while((s32[]{:T(128)}, f32[2,256]{1,0:T(2,128)S(1)}, ...), condition=%wide.region_9.10_spmd.clone, body=%wide.region_1.9_spmd.clone.sunk | while | flops 677055232 | bytes 22052092 | solution.py:180
  40.0 1.4 fusion.118
  42.5 5.8 %conditional.3 = ((f32[2,256]{1,0:T(2,128)S(1)}, f32[2,256]{1,0:T(2,128)S(1)}, f32[2,256,128]{2,1,0:T(8,128)S(1)}, f32[2,256]{1,0:T(2,128)S(1)}, f32[2,256]{1,0:T(2,128)}, /*index=5*/f32[2,256,64]{1,2,0:T(8,128)S(1)})) conditional(s32[]{:T(128)} %convert_element_type.241, (f32[2,256]{1,0:T(2,128)S(1)}, f32[2,256]{1,0:T(2,128)S(1)}, ...), branch_computations={%region_3.0_spmd, %region_4.8_spmd} | conditional | flops 677054720 | bytes 22046484 | solution.py:178
  42.6 1.4 convolution_convert_fusion.1
  48.4 1.4 fusion.118
  50.9 5.8 %conditional.3 = ((f32[2,256]{1,0:T(2,128)S(1)}, f32[2,256]{1,0:T(2,128)S(1)}, f32[2,256,128]{2,1,0:T(8,128)S(1)}, f32[2,256]{1,0:T(2,128)S(1)}, f32[2,256]{1,0:T(2,128)}, /*index=5*/f32[2,256,64]{1,2,0:T(8,128)S(1)})) conditional(s32[]{:T(128)} %convert_element_type.241, (f32[2,256]{1,0:T(2,128)S(1)}, f32[2,256]{1,0:T(2,128)S(1)}, ...), branch_computations={%region_3.0_spmd, %region_4.8_spmd} | conditional | flops 677054720 | bytes 22046484 | solution.py:178
  50.9 1.4 convolution_convert_fusion.1
  57.5 2.0 fusion.90
  59.5 2.1 fusion.36
  63.1 29.6 %reduce-scatter.3.cloned.1.call-done = bf16[64,4096]{1,0:T(8,128)(2,1)} async-done(((bf16[256,4096]{1,0:T(8,128)(2,1)}), bf16[64,4096]{1,0:T(8,128)(2,1)}) %reduce-scatter.3.cloned.1.call-update) | async-done | bytes 524304 | tf_op jit(solution)/shard_map/reduce_scatter | solution.py:183
  92.7 1.3 fusion.61
  94.1 1.2 fusion.63
  95.3 2.1 convolution_convert_fusion.6
  97.4 6.5 %all-to-all-start = ((bf16[16,16,4096]{2,1,0:T(8,128)(2,1)}), bf16[16,16,4096]{2,1,0:T(8,128)(2,1)}, u32[]{:S(2)}, u32[]{:S(2)}) async-start(bf16[16,16,4096]{2,1,0:T(8,128)(2,1)} %bitcast.126), calls=%async_computation.2 | async-start | bytes 4194304 | tf_op jit(solution)/shard_map/all_to_all | solution.py:223
  104.6 31.0 %all-gather.5.cloned.1.call-done = bf16[256,4096]{1,0:T(8,128)(2,1)} async-done(((bf16[64,4096]{1,0:T(8,128)(2,1)}), bf16[256,4096]{1,0:T(8,128)(2,1)}) %all-gather.5.cloned.1.call-update) | async-done | bytes 2097168 | tf_op jit(solution)/shard_map/all_gather | solution.py:194
  135.6 2.5 %fusion.91 = f32[256,128]{1,0:T(8,128)S(1)} fusion(bf16[256,4096]{1,0:T(8,128)(2,1)} %all-gather.5.cloned.1.call-done, bf16[4096,128]{1,0:T(8,128)(2,1)} %param.38), kind=kOutput, calls=%fused_computation.134 | convolution fusion | flops 268435456 | bytes 3276800 | tf_op jit(solution)/shard_map/dot_general | solution.py:195
  138.1 12.4 %all-to-all-done = bf16[16,16,4096]{2,1,0:T(8,128)(2,1)} async-done(((bf16[16,16,4096]{2,1,0:T(8,128)(2,1)}), bf16[16,16,4096]{2,1,0:T(8,128)(2,1)}, u32[]{:S(2)}, u32[]{:S(2)}) %all-to-all-start) | async-done | bytes 2097184 | tf_op jit(solution)/shard_map/all_to_all | solution.py:223
  150.5 2.8 %fusion.42 = f32[16,1,16,192]{3,2,0,1:T(8,128)S(1)} fusion(bf16[16,16,4096]{2,1,0:T(8,128)(2,1)} %all-to-all-done, bf16[1,4096,192]{1,2,0:T(8,128)(2,1)} %param.41), kind=kOutput, calls=%fused_computation.66 | convolution fusion | flops 402653184 | bytes 3866624 | tf_op jit(solution)/shard_map/sxcd,xdf->sxcf/dot_general | solution.py:226
  153.3 6.2 %convolution_convert_fusion.5 = bf16[16,16,4096]{2,1,0:T(8,128)(2,1)} fusion(bf16[1,192,4096]{2,1,0:T(8,128)(2,1)} %param.43, bf16[16,16,4096]{2,1,0:T(8,128)(2,1)} %all-to-all-done, bf16[1,4096,192]{1,2,0:T(8,128)(2,1)} %param.42, f32[16,1,16,192]{3,2,0,1:T(8,128)S(1)} %fusion.42), kind=kOutput, calls=%fused_computation.55 | convolution fusion | flops 806649856 | bytes 7536640 | tf_op jit(solution)/shard_map/sxcf,xfd->sxcd/dot_general | solution.py:231
  159.5 5.7 %all-to-all-start.1 = ((bf16[16,16,4096]{2,1,0:T(8,128)(2,1)}), bf16[16,16,4096]{2,1,0:T(8,128)(2,1)}, u32[]{:S(2)}, u32[]{:S(2)}) async-start(bf16[16,16,4096]{2,1,0:T(8,128)(2,1)} %convolution_convert_fusion.5), calls=%async_computation.3 | async-start | bytes 4194304 | tf_op jit(solution)/shard_map/all_to_all | solution.py:234
  165.5 4.8 %convolution_convert_fusion.4 = bf16[256,4096]{1,0:T(8,128)(2,1)} fusion(bf16[128,4096]{1,0:T(8,128)(2,1)} %param.40, bf16[256,4096]{1,0:T(8,128)(2,1)} %all-gather.5.cloned.1.call-done, bf16[4096,128]{1,0:T(8,128)(2,1)} %param.39, f32[256,128]{1,0:T(8,128)S(1)} %fusion.91), kind=kOutput, calls=%fused_computation.53 | convolution fusion | flops 538116096 | bytes 6422528 | tf_op jit(solution)/shard_map/dot_general | solution.py:198
  171.1 40.8 %all-to-all-done.1 = bf16[16,16,4096]{2,1,0:T(8,128)(2,1)} async-done(((bf16[16,16,4096]{2,1,0:T(8,128)(2,1)}), bf16[16,16,4096]{2,1,0:T(8,128)(2,1)}, u32[]{:S(2)}, u32[]{:S(2)}) %all-to-all-start.1) | async-done | bytes 2097184 | tf_op jit(solution)/shard_map/all_to_all | solution.py:234
  211.8 5.0 %gather_fusion = bf16[128,4096]{1,0:T(8,128)(2,1)} fusion(bf16[256,4096]{1,0:T(8,128)(2,1)} %bitcast.31, s32[1024]{0:T(1024)S(1)} %pad_clamp_fusion), kind=kCustom, calls=%fused_computation | custom fusion | bytes 2097664 | tf_op jit(solution)/shard_map/gather | solution.py:237
  216.9 3.4 %reshape.229 = f32[64,2,4096]{2,1,0:T(2,128)} reshape(bf16[128,4096]{1,0:T(8,128)(2,1)} %gather_fusion) | data formatting | bytes 3145728 | tf_op jit(solution)/shard_map/convert_element_type | solution.py:239
  220.2 5.7 %multiply_reduce_fusion = f32[64,4096]{1,0:T(8,128)} fusion(f32[64,2,4096]{2,1,0:T(2,128)} %reshape.229, f32[64,2]{1,0:T(8,128)S(1)} %copy.54), kind=kLoop, calls=%fused_computation.57 | loop fusion | flops 786432 | bytes 3146240 | tf_op jit(solution)/shard_map/reduce_sum | solution.py:238
  226.0 2.4 %fusion.65 = bf16[64,4096]{1,0:T(8,128)(2,1)} fusion(f32[64,4096]{1,0:T(8,128)} %multiply_reduce_fusion, bf16[64,4096]{1,0:T(8,128)(2,1)} %reduce-scatter.5.cloned.1.call-done, bf16[64,4096]{1,0:T(8,128)(2,1)S(1)} %copy-done.6, bf16[64,4096]{1,0:T(8,128)(2,1)S(1)} %copy-done.5), kind=kLoop, calls=%fused_computation.79 | loop fusion | flops 2359296 | bytes 3145728 | tf_op jit(solution)/shard_map/convert_element_type | solution.py:243
  (130 shorter events, 17.6 us)
Async XLA Ops:
  6.5 53.0 %copy-start = (bf16[256,4096]{1,0:T(8,128)(2,1)S(1)}, bf16[256,4096]{1,0:T(8,128)(2,1)}, u32[]{:S(2)}) copy-start(bf16[256,4096]{1,0:T(8,128)(2,1)} %param.34) | copy-start | bytes 6291460
  6.5 32.2 %all-gather.3.cloned.1.call-start = ((), (), s32[]{:S(2)}) async-start(), calls=%async_computation.4 | async-start | bytes 1310720 | tf_op jit(solution)/shard_map/all_gather | solution.py:120
  7.8 32.2 %copy-start.2 = (bf16[512,256]{1,0:T(8,128)(2,1)S(1)}, bf16[512,256]{1,0:T(8,128)(2,1)}, u32[]{:S(2)}) copy-start(bf16[512,256]{1,0:T(8,128)(2,1)} %param.29) | copy-start | bytes 786436
  7.8 32.2 %copy-start.3 = (bf16[512,256]{1,0:T(8,128)(2,1)S(1)}, bf16[512,256]{1,0:T(8,128)(2,1)}, u32[]{:S(2)}) copy-start(bf16[512,256]{1,0:T(8,128)(2,1)} %param.30) | copy-start | bytes 786436
  7.8 32.2 %copy-start.7 = (bf16[512,128]{1,0:T(8,128)(2,1)S(1)}, bf16[512,128]{1,0:T(8,128)(2,1)}, u32[]{:S(2)}) copy-start(bf16[512,128]{1,0:T(8,128)(2,1)} %param.31) | copy-start | bytes 393220
  7.8 32.2 %copy-start.8 = (bf16[512,128]{1,0:T(8,128)(2,1)S(1)}, bf16[512,128]{1,0:T(8,128)(2,1)}, u32[]{:S(2)}) copy-start(bf16[512,128]{1,0:T(8,128)(2,1)} %param.32) | copy-start | bytes 393220
  9.7 83.0 %reduce-scatter.3.cloned.1.call-start = ((), (), s32[]{:S(2)}) async-start(), calls=%async_computation.5 | async-start | bytes 2621440 | tf_op jit(solution)/shard_map/reduce_scatter | solution.py:183
  42.6 1.8 copy-start.14
  42.6 2.0 copy-start.10
  44.0 1.2 copy-start.1
  44.0 1.5 copy-start.9
  44.6 1.4 copy-start.11
  45.9 0.8 copy-start.12
  46.8 1.6 copy-start.13
  50.9 1.8 copy-start.14
  50.9 2.0 copy-start.10
  52.4 1.2 copy-start.1
  52.4 1.5 copy-start.9
  52.9 1.4 copy-start.11
  54.3 0.8 copy-start.12
  55.1 1.5 copy-start.13
  61.7 0.7 copy-start.16
  61.7 31.1 %copy-start.5 = (bf16[64,4096]{1,0:T(8,128)(2,1)S(1)}, bf16[64,4096]{1,0:T(8,128)(2,1)}, u32[]{:S(2)}) copy-start(bf16[64,4096]{1,0:T(8,128)(2,1)} %param.36) | copy-start | bytes 1572868
  61.7 32.4 %copy-start.15 = (f32[4096]{0:T(1024)S(1)}, f32[4096]{0:T(1024)}, u32[]{:S(2)}) copy-start(f32[4096]{0:T(1024)} %param.37) | copy-start | bytes 49156
  95.3 2.1 copy-start.4
  97.4 53.1 %all-to-all-start = ((bf16[16,16,4096]{2,1,0:T(8,128)(2,1)}), bf16[16,16,4096]{2,1,0:T(8,128)(2,1)}, u32[]{:S(2)}, u32[]{:S(2)}) async-start(bf16[16,16,4096]{2,1,0:T(8,128)(2,1)} %bitcast.126), calls=%async_computation.2 | async-start | bytes 4194304 | tf_op jit(solution)/shard_map/all_to_all | solution.py:223
  103.9 31.7 %all-gather.5.cloned.1.call-start = ((), (), s32[]{:S(2)}) async-start(), calls=%async_computation.6 | async-start | bytes 2621440 | tf_op jit(solution)/shard_map/all_gather | solution.py:194
  159.5 52.3 %all-to-all-start.1 = ((bf16[16,16,4096]{2,1,0:T(8,128)(2,1)}), bf16[16,16,4096]{2,1,0:T(8,128)(2,1)}, u32[]{:S(2)}, u32[]{:S(2)}) async-start(bf16[16,16,4096]{2,1,0:T(8,128)(2,1)} %convolution_convert_fusion.5), calls=%async_computation.3 | async-start | bytes 4194304 | tf_op jit(solution)/shard_map/all_to_all | solution.py:234
  165.2 60.7 %reduce-scatter.5.cloned.1.call-start = ((), (), s32[]{:S(2)}) async-start(), calls=%async_computation.7 | async-start | bytes 2621440 | tf_op jit(solution)/shard_map/reduce_scatter | solution.py:199
  170.3 0.7 copy-start.17
  220.2 5.7 %copy-start.6 = (bf16[64,4096]{1,0:T(8,128)(2,1)S(1)}, bf16[64,4096]{1,0:T(8,128)(2,1)}, u32[]{:S(2)}) copy-start(bf16[64,4096]{1,0:T(8,128)(2,1)} %reduce-scatter.3.cloned.1.call-done) | copy-start | bytes 1572868
Sparse Core Ops, SparseCore 0:
  9.8 28.8 all-gather.2
  61.8 30.8 reduce-scatter.2
  106.2 29.2 all-gather.4
  170.4 34.1 reduce-scatter.4
where the time goes:
time: 237 us; the launch traced here: 235 us
  waiting for transfers between devices  126 us (53%)
  matrix products  32 us (14%)
  other arithmetic  21.7 us (9%)
  local copies, waits for them, and re-layouts  16.2 us (7%)
  between operations  13.4 us (6%)
  starting transfers between devices  12.5 us (5%)
  blocking collectives  11.6 us (5%)
    all_to_all x1, waiting for transfers between devices, body(): lax.all_to_all(finished.reshape(incoming.shape), ('sp', 'tp'), split_axis...  40.8 us
    all_gather x1, waiting for transfers between devices, body(): piece = lax.all_gather(normed, 'tp', axis=0, tiled=True)  31 us
    reduce_scatter x1, waiting for transfers between devices, body(): lax.psum_scatter((jnp.dot(wide_mix, out_wide, preferred_element_type=jnp....  29.6 us
    all_to_all x1, waiting for transfers between devices, body(): lax.all_to_all(outgoing, ('sp', 'tp'), split_axis=0, concat_axis=0, tiled...  12.4 us
    all_gather x1, blocking collectives, body(): lax.all_gather(turned_key, 'sp', axis=0, tiled=True)  11.6 us
    all_gather x1, waiting for transfers between devices, body(): lax.all_gather(normed_latent, 'sp', axis=0, tiled=True)  11.3 us
    all_to_all x1, starting transfers between devices, body(): lax.all_to_all(outgoing, ('sp', 'tp'), split_axis=0, concat_axis=0, tiled...  6.47 us
    dot_general x1, matrix products, body(): jnp.einsum('sxcf,xfd->sxcd', active, expert_down, preferred_element_type=...  6.24 us
  transfers between devices with their start and end apart: 6, of which 5 were waited for; matrix products, arithmetic and copies ran while one was open for 12% of the time, Pallas kernels for 0%

commit v1 on v0

--- a/solution.py
+++ b/solution.py
@@ -3,11 +3,255 @@
 import jax
 import jax.numpy as jnp
 from jax import lax
+from jax.experimental import pallas as pl
+from jax.experimental.pallas import tpu as pltpu
 from jax.sharding import PartitionSpec as P
 
 ROPE = 64
 WIDE_HEAD_SIZE = 128
 NARROW_HEAD_SIZE = 64
+
+
+MESH = pl.DeviceIdType.MESH
+VMEM = pl.BlockSpec(memory_space=pltpu.VMEM)
+
+
+def flip(index, bits):
+    mask = 1
+    while mask <= bits:
+        if bits & mask:
+            index = index + mask - 2 * mask * ((index // mask) % 2)
+        mask *= 2
+    return index
+
+
+def masks_of(count):
+    return [1 << k for k in range(count.bit_length() - 1)]
+
+
+def low_bit(number):
+    return number & -number
+
+
+def greet(partners):
+    barrier = pltpu.get_barrier_semaphore()
+    for partner in partners:
+        pl.semaphore_signal(barrier, inc=1, device_id=partner, device_id_type=MESH)
+    pl.semaphore_wait(barrier, len(partners))
+
+
+def doubling_order(count):
+    return sorted(range(count), key=lambda d: (bin(d).count("1"), -d))
+
+
+def remote(src, dst, send_sem, recv_sem, target):
+    return pltpu.make_async_remote_copy(
+        src_ref=src,
+        dst_ref=dst,
+        send_sem=send_sem,
+        recv_sem=recv_sem,
+        device_id=target,
+        device_id_type=MESH,
+    )
+
+
+def spread_kernel(n_sp, n_tp, x_ref, out_ref, z_send, z_recv, t_send, t_recv, own_sem):
+    sp, tp = lax.axis_index("sp"), lax.axis_index("tp")
+    tok = x_ref.shape[0]
+    part = tok // n_tp
+    targets = [{"sp": lax.rem(sp + r, n_sp)} for r in range(1, n_sp)]
+    greet(targets + [{"tp": flip(tp, m)} for m in masks_of(n_tp)])
+
+    def rows(block, member):
+        return pl.ds(pl.multiple_of(block * tok + member * part, part), part)
+
+    own = pltpu.make_async_copy(
+        x_ref, out_ref.at[pl.ds(pl.multiple_of(sp * tok, tok), tok)], own_sem
+    )
+    sends = []
+    for r in range(1, n_sp):
+        copy = remote(
+            x_ref.at[pl.ds(pl.multiple_of(tp * part, part), part)],
+            out_ref.at[rows(sp, tp)],
+            z_send.at[r],
+            z_recv.at[r],
+            targets[r - 1],
+        )
+        copy.start()
+        sends.append(copy)
+    own.start()
+
+    def piece(r, d):
+        return out_ref.at[rows(lax.rem(sp + n_sp - r, n_sp), flip(tp, d))]
+
+    for d in doubling_order(n_tp):
+        for r in range(1, n_sp):
+            block = piece(r, d)
+            if d == 0:
+                sends[r - 1].wait_recv()
+            else:
+                remote(
+                    block, block, t_send.at[r, d], t_recv.at[r, d], {"tp": flip(tp, low_bit(d))}
+                ).wait_recv()
+            for mask in reversed(masks_of(low_bit(d) if d else n_tp)):
+                copy = remote(
+                    block,
+                    block,
+                    t_send.at[r, d + mask],
+                    t_recv.at[r, d + mask],
+                    {"tp": flip(tp, mask)},
+                )
+                copy.start()
+                sends.append(copy)
+    for copy in sends:
+        copy.wait_send()
+    own.wait()
+
+
+def spread(x, n_sp, n_tp):
+    tok, width = x.shape
+    return pl.pallas_call(
+        lambda *refs: spread_kernel(n_sp, n_tp, *refs),
+        out_shape=jax.ShapeDtypeStruct((n_sp * tok, width), x.dtype),
+        in_specs=[VMEM],
+        out_specs=VMEM,
+        scratch_shapes=[
+            pltpu.SemaphoreType.DMA((n_sp,)),
+            pltpu.SemaphoreType.DMA((n_sp,)),
+            pltpu.SemaphoreType.DMA((n_sp, n_tp)),
+            pltpu.SemaphoreType.DMA((n_sp, n_tp)),
+            pltpu.SemaphoreType.DMA,
+        ],
+        compiler_params=pltpu.CompilerParams(collective_id=0, has_side_effects=True),
+        cost_estimate=pl.CostEstimate(flops=0, bytes_accessed=30_000_000, transcendentals=0),
+    )(x)
+
+
+def gather_kernel(n_tp, pieces, x_ref, out_ref, send, recv, own_sem):
+    tp = lax.axis_index("tp")
+    rows, width = x_ref.shape
+    part = width // pieces
+    greet([{"tp": flip(tp, m)} for m in masks_of(n_tp)])
+
+    def block(d, c):
+        start = pl.multiple_of(flip(tp, d) * rows, rows)
+        return out_ref.at[pl.ds(start, rows), pl.ds(c * part, part)]
+
+    own = pltpu.make_async_copy(
+        x_ref, out_ref.at[pl.ds(pl.multiple_of(tp * rows, rows), rows)], own_sem
+    )
+    sends = []
+    for d in doubling_order(n_tp):
+        for c in range(pieces):
+            source = x_ref.at[:, pl.ds(c * part, part)] if d == 0 else block(d, c)
+            if d:
+                remote(
+                    source, source, send.at[d, c], recv.at[d, c], {"tp": flip(tp, low_bit(d))}
+                ).wait_recv()
+            for mask in reversed(masks_of(low_bit(d) if d else n_tp)):
+                copy = remote(
+                    source,
+                    block(d, c),
+                    send.at[d + mask, c],
+                    recv.at[d + mask, c],
+                    {"tp": flip(tp, mask)},
+                )
+                copy.start()
+                sends.append(copy)
+        if d == 0:
+            own.start()
+    for copy in sends:
+        copy.wait_send()
+    own.wait()
+
+
+def gather_rows(x, n_tp, pieces=2):
+    rows, width = x.shape
+    return pl.pallas_call(
+        lambda *refs: gather_kernel(n_tp, pieces, *refs),
+        out_shape=jax.ShapeDtypeStruct((n_tp * rows, width), x.dtype),
+        in_specs=[VMEM],
+        out_specs=VMEM,
+        scratch_shapes=[
+            pltpu.SemaphoreType.DMA((n_tp, pieces)),
+            pltpu.SemaphoreType.DMA((n_tp, pieces)),
+            pltpu.SemaphoreType.DMA,
+        ],
+        compiler_params=pltpu.CompilerParams(collective_id=1, has_side_effects=True),
+        cost_estimate=pl.CostEstimate(flops=0, bytes_accessed=40_000_000, transcendentals=0),
+    )(x)
+
+
+def scatter_kernel(n_tp, pieces, pairs, *refs):
+    lefts, rights = refs[:pairs], refs[pairs : 2 * pairs]
+    out_ref, sent, got, send, recv = refs[2 * pairs :]
+    tp = lax.axis_index("tp")
+    rows, width = out_ref.shape
+    part = width // pieces
+    greet([{"tp": flip(tp, m)} for m in masks_of(n_tp)])
+    copies = {}
+
+    def product(d, c):
+        start = pl.multiple_of(flip(tp, d) * rows, rows)
+        total = None
+        for left, right in zip(lefts, rights):
+            term = jnp.dot(
+                left[pl.ds(start, rows), :],
+                right[:, pl.ds(c * part, part)],
+                preferred_element_type=jnp.float32,
+            )
+            total = term if total is None else total + term
+        return total
+
+    def summed(d, c, below):
+        total = product(d, c)
+        if below > 1:
+            total = total.astype(jnp.bfloat16).astype(jnp.float32)
+        for mask in masks_of(below):
+            copies[d + mask, c].wait_recv()
+            total = total + got[d + mask, :, pl.ds(c * part, part)].astype(jnp.float32)
+        return total
+
+    def pass_on(mask, c):
+        for d in range(mask, n_tp, 2 * mask):
+            sent[d, :, pl.ds(c * part, part)] = summed(d, c, mask).astype(jnp.bfloat16)
+            copies[d, c] = remote(
+                sent.at[d, :, pl.ds(c * part, part)],
+                got.at[d, :, pl.ds(c * part, part)],
+                send.at[d, c],
+                recv.at[d, c],
+                {"tp": flip(tp, mask)},
+            )
+            copies[d, c].start()
+
+    masks = masks_of(n_tp)
+    for step in range(pieces + len(masks) - 1):
+        for stage, mask in enumerate(masks):
+            if 0 <= step - stage < pieces:
+                pass_on(mask, step - stage)
+    for c in range(pieces):
+        out_ref[:, pl.ds(c * part, part)] = summed(0, c, n_tp)
+    for copy in copies.values():
+        copy.wait_send()
+
+
+def dot_scatter(lefts, rights, n_tp, collective, pieces=4):
+    rows, width = lefts[0].shape[0] // n_tp, rights[0].shape[1]
+    pairs = len(lefts)
+    return pl.pallas_call(
+        lambda *refs: scatter_kernel(n_tp, pieces, pairs, *refs),
+        out_shape=jax.ShapeDtypeStruct((rows, width), jnp.float32),
+        in_specs=[VMEM] * (2 * pairs),
+        out_specs=VMEM,
+        scratch_shapes=[
+            pltpu.VMEM((n_tp, rows, width), jnp.bfloat16),
+            pltpu.VMEM((n_tp, rows, width), jnp.bfloat16),
+            pltpu.SemaphoreType.DMA((n_tp, pieces)),
+            pltpu.SemaphoreType.DMA((n_tp, pieces)),
+        ],
+        compiler_params=pltpu.CompilerParams(collective_id=collective, has_side_effects=True),
+        cost_estimate=pl.CostEstimate(flops=0, bytes_accessed=40_000_000, transcendentals=0),
+    )(*lefts, *rights)
 
 
 EPS = 1e-06
@@ -116,10 +360,13 @@
     initial = empty_state(wide_local, tok_dev, WIDE_HEAD_SIZE) + empty_state(
         narrow_local, tok_dev, NARROW_HEAD_SIZE
     )
-    pieces = (
-        lax.all_gather(normed_latent, "sp", axis=0, tiled=True),
-        lax.all_gather(turned_key, "sp", axis=0, tiled=True),
-    )
+    n_sp, n_tp = lax.axis_size("sp"), lax.axis_size("tp")
+    latent_width = latent.shape[1]
+    packed = jnp.concatenate(
+        [normed_latent, jnp.pad(turned_key, ((0, 0), (0, -turned_key.shape[1] % 128)))], axis=1
+    )
+    packed = spread(packed, n_sp, n_tp)
+    pieces = (packed[:, :latent_width], packed[:, latent_width : latent_width + ROPE])
     indices = jnp.arange(pieces[0].shape[0], dtype=jnp.int32)
     placing = lambda positions: positions
     latent_rows, turned_rows = pieces
@@ -180,25 +427,14 @@
     final = lax.fori_loop(0, length_rows // block, one_block, initial)
     wide_mix = finish(final[:3])
     narrow_mix = finish(final[3:])
-    projected = lax.psum_scatter(
-        (
-            jnp.dot(wide_mix, out_wide, preferred_element_type=jnp.float32)
-            + jnp.dot(narrow_mix, out_narrow, preferred_element_type=jnp.float32)
-        ).astype(jnp.bfloat16),
-        "tp",
-        scatter_dimension=0,
-        tiled=True,
-    ).astype(jnp.float32)
+    projected = dot_scatter((wide_mix, narrow_mix), (out_wide, out_narrow), n_tp, 2)
     stream = (residual.astype(jnp.float32) + projected).astype(jnp.bfloat16)
     normed = rms_scale(stream.astype(jnp.float32), ffn_gain).astype(jnp.bfloat16)
-    piece = lax.all_gather(normed, "tp", axis=0, tiled=True)
+    piece = gather_rows(normed, n_tp)
     gate_part = jnp.dot(piece, shared_gate, preferred_element_type=jnp.float32)
     up_part = jnp.dot(piece, shared_up, preferred_element_type=jnp.float32)
     active = (jax.nn.silu(gate_part) * up_part).astype(jnp.bfloat16)
-    shared_terms = jnp.dot(active, shared_down, preferred_element_type=jnp.float32)
-    shared = lax.psum_scatter(
-        shared_terms.astype(jnp.bfloat16), "tp", scatter_dimension=0, tiled=True
-    ).astype(jnp.float32)
+    shared = dot_scatter((active,), (shared_down,), n_tp, 3)
     rows_here, top_count = routes.shape
     local_experts = expert_gate.shape[0]
     experts_all = local_experts * lax.axis_size(("sp", "tp"))
@@ -234,12 +470,15 @@
     returned = lax.all_to_all(
         finished.reshape(incoming.shape), ("sp", "tp"), split_axis=0, concat_axis=0, tiled=True
     )
-    picked = returned.reshape(experts_all * capacity, model_width)[target]
-    routed = jnp.sum(
-        picked.reshape(rows_here, top_count, model_width).astype(jnp.float32)
-        * route_weights[:, :, None],
-        axis=1,
-    )
+    slot_rows = returned.reshape(experts_all * capacity, model_width)
+    by_choice = target.reshape(rows_here, top_count)
+    routed = jnp.zeros((rows_here, model_width), jnp.float32)
+    for choice in range(top_count):
+        hot = by_choice[:, choice : choice + 1] == jnp.arange(experts_all * capacity)[None, :]
+        picked = jnp.dot(
+            hot.astype(jnp.bfloat16), slot_rows, preferred_element_type=jnp.float32
+        )
+        routed = routed + picked * route_weights[:, choice : choice + 1]
     return (stream.astype(jnp.float32) + shared + routed).astype(jnp.bfloat16)
 
 

time: 237 us -> 213 us (0.90)
  waiting for transfers between devices: 126 us -> 0.01 us
  Pallas kernels: 0 us -> 92.1 us
  blocking collectives: 11.6 us -> 52.8 us
  between operations: 13.4 us -> 0.37 us
  starting transfers between devices: 12.5 us -> 5.74 us
  matrix products: 32 us -> 25.7 us
  other arithmetic: 21.7 us -> 15.5 us
    pallas_call x0 -> x4, Pallas kernels: none -> 92.1 us  [the longest x2 41.5 us: dot_scatter(): pl.pallas_call(lambda *refs: scatter_kernel(n_tp, pieces, pairs, *refs),...]
    all_to_all x0 -> x1, blocking collectives: none -> 52.8 us  [body(): lax.all_to_all(outgoing, ('sp', 'tp'), split_axis=0, concat_axis=0, tiled...]
    all_gather x2 -> x0, waiting for transfers between devices: 42.2 us -> none  [the longest x1 31 us: body(): piece = lax.all_gather(normed, 'tp', axis=0, tiled=True)]
    all_to_all x1, waiting for transfers between devices: 40.8 us -> 0.01 us  [body(): lax.all_to_all(finished.reshape(incoming.shape), ('sp', 'tp'), split_axis...]
    reduce_scatter x2 -> x0, waiting for transfers between devices: 29.6 us -> none  [the longest x1 29.6 us: body(): lax.psum_scatter((jnp.dot(wide_mix, out_wide, preferred_element_type=jnp....]
    all_to_all x1 -> x0, waiting for transfers between devices: 12.4 us -> none  [body(): lax.all_to_all(outgoing, ('sp', 'tp'), split_axis=0, concat_axis=0, tiled...]
    all_gather x1 -> x0, blocking collectives: 11.6 us -> none  [body(): lax.all_gather(turned_key, 'sp', axis=0, tiled=True)]
    all_to_all x1 -> x0, starting transfers between devices: 6.47 us -> none  [body(): lax.all_to_all(outgoing, ('sp', 'tp'), split_axis=0, concat_axis=0, tiled...]
  transfers between devices with their start and end apart: 6 -> 1, of which waited for: 5 -> 0; matrix products, arithmetic and copies ran while one was open for 12% -> 2% of each run, Pallas kernels for 0% -> 26%
where the time goes in v1:
time: 213 us; the launch traced here: 212 us
  Pallas kernels  92.1 us (43%)
  blocking collectives  52.8 us (25%)
  matrix products  25.7 us (12%)
  local copies, waits for them, and re-layouts  18.2 us (9%)
  other arithmetic  15.5 us (7%)
  starting transfers between devices  5.74 us (3%)
    all_to_all x1, blocking collectives, body(): lax.all_to_all(outgoing, ('sp', 'tp'), split_axis=0, concat_axis=0, tiled...  52.8 us
    pallas_call x2, Pallas kernels, dot_scatter(): pl.pallas_call(lambda *refs: scatter_kernel(n_tp, pieces, pairs, *refs),...  41.5 us
    pallas_call x1, Pallas kernels, gather_rows(): pl.pallas_call(lambda *refs: gather_kernel(n_tp, pieces, *refs), out_shap...  32.5 us
    pallas_call x1, Pallas kernels, spread(): pl.pallas_call(lambda *refs: spread_kernel(n_sp, n_tp, *refs), out_shape=...  18 us
    unnamed x32, local copies, waits for them, and re-layouts  8.46 us
    dot_general x1, matrix products, body(): jnp.einsum('sxcf,xfd->sxcd', active, expert_down, preferred_element_type=...  5.75 us
    all_to_all x1, starting transfers between devices, body(): lax.all_to_all(finished.reshape(incoming.shape), ('sp', 'tp'), split_axis...  5.74 us
    dot_general x2, matrix products, body(): jnp.dot(hot.astype(jnp.bfloat16), slot_rows, preferred_element_type=jnp.f...  5.23 us
  transfers between devices with their start and end apart: 1, of which 0 were waited for; matrix products, arithmetic and copies ran while one was open for 2% of the time, Pallas kernels for 26%

profile of v1, /device:TPU:27, one launch (start us, length us, event | category | flops | bytes accessed | tf_op | source)
XLA Modules:
  0.0 212.1 jit_solution(7684956934899067993)
XLA Ops:
  0.0 1.0 copy.75
  1.0 1.1 fusion.66
  2.1 1.3 multiply_cosine_fusion
  3.5 1.1 fusion.68
  5.4 18.0 %shard_map.199 = bf16[1024,640]{1,0:T(8,128)(2,1)} custom-call(bf16[256,640]{1,0:T(8,128)(2,1)} %pad_maximum_fusion.refs_0_), custom_call_target="tpu_custom_call" | custom-call | bytes 30000000 | tf_op jit(solution)/shard_map/pallas_call | solution.py:113
  23.4 1.3 slice.50
  24.8 1.8 copy.77
  27.4 1.6 slice.66
  29.0 1.6 copy.78
  30.6 1.6 copy.79
  32.2 1.7 copy.80
  33.8 1.6 slice_convert_fusion
  36.2 1.7 copy.81
  40.7 16.0 %while.24 = (s32[]{:T(128)}, f32[2,256]{1,0:T(2,128)S(1)}, f32[2,256]{1,0:T(2,128)S(1)}, f32[2,256,128]{2,1,0:T(8,128)S(1)}, f32[2,256]{1,0:T(2,128)S(1)}, /*ind...) while((s32[]{:T(128)}, f32[2,256]{1,0:T(2,128)S(1)}, ...), condition=%wide.region_9.10_spmd.clone, body=%wide.region_1.9_spmd.clone.sunk | while | flops 677055232 | bytes 19430200 | solution.py:427
  40.7 1.4 fusion.112
  43.2 5.5 %conditional.3 = ((f32[2,256]{1,0:T(2,128)S(1)}, f32[2,256]{1,0:T(2,128)S(1)}, f32[2,256,128]{2,1,0:T(8,128)S(1)}, f32[2,256]{1,0:T(2,128)S(1)}, f32[2,256]{1,0:T(2,128)}, /*index=5*/f32[2,256,64]{1,2,0:T(8,128)S(1)})) conditional(s32[]{:T(128)} %convert_element_type.188, (f32[2,256]{1,0:T(2,128)S(1)}, f32[2,256]{1,0:T(2,128)S(1)}, ...), branch_computations={%region_3.3_spmd, %region_4.8_spmd} | conditional | flops 677054720 | bytes 19424592 | solution.py:425
  43.6 1.3 convolution_bitcast_fusion
  48.7 1.4 fusion.112
  51.2 5.5 %conditional.3 = ((f32[2,256]{1,0:T(2,128)S(1)}, f32[2,256]{1,0:T(2,128)S(1)}, f32[2,256,128]{2,1,0:T(8,128)S(1)}, f32[2,256]{1,0:T(2,128)S(1)}, f32[2,256]{1,0:T(2,128)}, /*index=5*/f32[2,256,64]{1,2,0:T(8,128)S(1)})) conditional(s32[]{:T(128)} %convert_element_type.188, (f32[2,256]{1,0:T(2,128)S(1)}, f32[2,256]{1,0:T(2,128)S(1)}, ...), branch_computations={%region_3.3_spmd, %region_4.8_spmd} | conditional | flops 677054720 | bytes 19424592 | solution.py:425
  51.6 1.3 convolution_bitcast_fusion
  58.9 18.8 %shard_map.200 = f32[64,4096]{1,0:T(8,128)} custom-call(bf16[256,256]{1,0:T(8,128)(2,1)} %copy_bitcast_fusion.refs_0_, bf16[256,128]{1,0:T(8,128)(2,1)} %copy.84.refs_1_, bf16[256,4096]{1,0:T(8,128)(2,1)} %refs_2_.1, bf16[128,4096]{1,0:T(8,128)(2,1)} %refs_3_.1), custom_call_target="tpu_custom_call" | custom-call | bytes 40000000 | tf_op jit(solution)/shard_map/pallas_call | solution.py:241
  77.8 1.5 fusion.63
  81.0 52.8 %all_to_all.10 = bf16[16,16,4096]{2,1,0:T(8,128)(2,1)S(1)} all-to-all(bf16[16,16,4096]{2,1,0:T(8,128)(2,1)S(1)} %bitcast.128), channel_id=1, replica_groups=mesh['grp'=2,'sp'=4,'tp'=4] {'sp','tp'}, dimensions={0} | all-to-all | bytes 4194304 | tf_op jit(solution)/shard_map/all_to_all | solution.py:459
  133.8 1.3 copy-done.12
  135.9 5.7 %convolution_convert_fusion.4 = bf16[16,16,4096]{2,1,0:T(8,128)(2,1)} fusion(bf16[1,192,4096]{2,1,0:T(8,128)(2,1)S(1)} %copy-done, bf16[16,16,4096]{2,1,0:T(8,128)(2,1)} %copy-done.12, bf16[1,4096,192]{1,2,0:T(8,128)(2,1)} %param.42, f32[16,1,16,192]{3,2,0,1:T(8,128)S(1)} %fusion.44), kind=kOutput, calls=%fused_computation.51 | convolution fusion | flops 806649856 | bytes 7536640 | tf_op jit(solution)/shard_map/sxcf,xfd->sxcd/dot_general | solution.py:467
  141.7 5.7 %all-to-all-start.1 = ((bf16[16,16,4096]{2,1,0:T(8,128)(2,1)}), bf16[16,16,4096]{2,1,0:T(8,128)(2,1)}, u32[]{:S(2)}, u32[]{:S(2)}) async-start(bf16[16,16,4096]{2,1,0:T(8,128)(2,1)} %convolution_convert_fusion.4), calls=%async_computation.1 | async-start | bytes 4194304 | tf_op jit(solution)/shard_map/all_to_all | solution.py:470
  147.4 32.5 %shard_map.201 = bf16[256,4096]{1,0:T(8,128)(2,1)} custom-call(bf16[64,4096]{1,0:T(8,128)(2,1)} %copy-done.5), custom_call_target="tpu_custom_call" | custom-call | bytes 40000000 | tf_op jit(solution)/shard_map/pallas_call | solution.py:170
  180.0 2.7 %fusion.87 = f32[256,128]{1,0:T(8,128)S(1)} fusion(bf16[256,4096]{1,0:T(8,128)(2,1)} %shard_map.201, bf16[4096,128]{1,0:T(8,128)(2,1)} %param.38), kind=kOutput, calls=%fused_computation.133 | convolution fusion | flops 268435456 | bytes 3276800 | tf_op jit(solution)/shard_map/dot_general | solution.py:434
  182.7 1.3 fusion.59.refs_0_
  184.1 22.7 %shard_map.202 = f32[64,4096]{1,0:T(8,128)} custom-call(bf16[256,128]{1,0:T(8,128)(2,1)} %fusion.59.refs_0_, bf16[128,4096]{1,0:T(8,128)(2,1)} %refs_1_.1), custom_call_target="tpu_custom_call" | custom-call | bytes 40000000 | tf_op jit(solution)/shard_map/pallas_call | solution.py:241
  206.8 2.2 %convolution_multiply_fusion.1 = f32[64,4096]{1,0:T(8,128)S(1)} fusion(bf16[256,4096]{1,0:T(8,128)(2,1)} %bitcast.31, f32[64]{0:T(128)S(1)} %get-tuple-element.708, s32[64]{0:T(128)S(1)} %get-tuple-element.706), kind=kOutput, calls=%fused_computation.55 | convolution fusion | flops 134496256 | bytes 3146240 | tf_op jit(solution)/shard_map/dot_general | solution.py:478
  209.0 3.0 %fusion.38 = bf16[64,4096]{1,0:T(8,128)(2,1)} fusion(f32[64,4096]{1,0:T(8,128)S(1)} %convolution_multiply_fusion.1, bf16[256,4096]{1,0:T(8,128)(2,1)} %bitcast.31, f32[64,4096]{1,0:T(8,128)S(1)} %copy-done.6, bf16[64,4096]{1,0:T(8,128)(2,1)S(1)} %get-tuple-element.684, f32[64]{0:T(128)S(1)} %get-tuple-element.707, s32[64]{0:T(128)S(1)} %get-tuple-element.705), kind=kOutput, calls=%fused_computation.57 | convolution fusion | flops 135806976 | bytes 5243392 | tf_op jit(solution)/shard_map/dot_general | solution.py:478
  (134 shorter events, 19.1 us)
Async XLA Ops:
  0.0 135.9 %copy-start = (bf16[1,192,4096]{2,1,0:T(8,128)(2,1)S(1)}, bf16[1,192,4096]{2,1,0:T(8,128)(2,1)}, u32[]{:S(2)}) copy-start(bf16[1,192,4096]{2,1,0:T(8,128)(2,1)} %param.43) | copy-start | bytes 4718596
  23.4 12.0 %slice-start = ((bf16[1024,640]{1,0:T(8,128)(2,1)}), bf16[1024,64]{1,0:T(8,128)(2,1)S(1)}, s32[]{:S(2)}) async-start(bf16[1024,640]{1,0:T(8,128)(2,1)} %shard_map.199), calls=%async_computation.2 | async-start | bytes 524288 | tf_op jit(solution)/shard_map/slice | solution.py:369
  24.8 15.9 %copy-start.2 = (bf16[512,256]{1,0:T(8,128)(2,1)S(1)}, bf16[512,256]{1,0:T(8,128)(2,1)}, u32[]{:S(2)}) copy-start(bf16[512,256]{1,0:T(8,128)(2,1)} %param.29) | copy-start | bytes 786436
  24.8 15.9 %copy-start.3 = (bf16[512,256]{1,0:T(8,128)(2,1)S(1)}, bf16[512,256]{1,0:T(8,128)(2,1)}, u32[]{:S(2)}) copy-start(bf16[512,256]{1,0:T(8,128)(2,1)} %param.30) | copy-start | bytes 786436
  43.2 1.7 copy-start.16
  43.2 1.9 copy-start.4
  43.2 1.9 copy-start.10
  43.6 1.9 copy-start.7
  43.6 2.2 %copy-start.9 = (bf16[256,2,64]{0,2,1:T(8,128)(2,1)S(1)}, bf16[256,2,64]{0,2,1:T(8,128)(2,1)}, u32[]{:S(2)}) copy-start(bf16[256,2,64]{0,2,1:T(8,128)(2,1)} %get-tuple-element.463) | copy-start | bytes 196612 | tf_op jit(solution)/shard_map/while/body/eval_jaxpr/cond
  45.1 1.1 copy-start.11
  46.2 0.9 copy-start.8
  47.0 1.6 copy-start.15
  51.2 1.7 copy-start.16
  51.2 1.9 copy-start.4
  51.2 1.9 copy-start.10
  51.6 1.9 copy-start.7
  51.6 2.2 %copy-start.9 = (bf16[256,2,64]{0,2,1:T(8,128)(2,1)S(1)}, bf16[256,2,64]{0,2,1:T(8,128)(2,1)}, u32[]{:S(2)}) copy-start(bf16[256,2,64]{0,2,1:T(8,128)(2,1)} %get-tuple-element.463) | copy-start | bytes 196612 | tf_op jit(solution)/shard_map/while/body/eval_jaxpr/cond
  53.1 1.1 copy-start.11
  54.2 0.8 copy-start.14
  54.2 0.9 copy-start.8
  55.0 1.6 copy-start.15
  58.9 18.8 %copy-start.13 = (bf16[64,4096]{1,0:T(8,128)(2,1)S(1)}, bf16[64,4096]{1,0:T(8,128)(2,1)}, u32[]{:S(2)}) copy-start(bf16[64,4096]{1,0:T(8,128)(2,1)} %param.36) | copy-start | bytes 1572868
  77.8 1.5 copy-start.18
  77.8 2.3 %copy-start.17 = (f32[4096]{0:T(1024)S(1)}, f32[4096]{0:T(1024)}, u32[]{:S(2)}) copy-start(f32[4096]{0:T(1024)} %param.37) | copy-start | bytes 49156
  80.2 53.6 %copy-start.5 = (bf16[64,4096]{1,0:T(8,128)(2,1)}, bf16[64,4096]{1,0:T(8,128)(2,1)S(1)}, u32[]{:S(2)}) copy-start(bf16[64,4096]{1,0:T(8,128)(2,1)S(1)} %fusion.65.refs_0_) | copy-start | bytes 1572868
  81.0 54.2 %copy-start.20 = (bf16[1,4096,192]{1,2,0:T(8,128)(2,1)S(1)}, bf16[1,4096,192]{1,2,0:T(8,128)(2,1)}, u32[]{:S(2)}) copy-start(bf16[1,4096,192]{1,2,0:T(8,128)(2,1)} %param.41) | copy-start | bytes 4718596
  133.8 1.3 copy-start.12
  141.7 65.1 %all-to-all-start.1 = ((bf16[16,16,4096]{2,1,0:T(8,128)(2,1)}), bf16[16,16,4096]{2,1,0:T(8,128)(2,1)}, u32[]{:S(2)}, u32[]{:S(2)}) async-start(bf16[16,16,4096]{2,1,0:T(8,128)(2,1)} %convolution_convert_fusion.4), calls=%async_computation.1 | async-start | bytes 4194304 | tf_op jit(solution)/shard_map/all_to_all | solution.py:470
  179.9 2.7 %copy-start.1 = (bf16[256,4096]{1,0:T(8,128)(2,1)S(1)}, bf16[256,4096]{1,0:T(8,128)(2,1)}, u32[]{:S(2)}) copy-start(bf16[256,4096]{1,0:T(8,128)(2,1)} %shard_map.201) | copy-start | bytes 6291460
  179.9 2.8 %copy-start.21 = (bf16[4096,128]{1,0:T(8,128)(2,1)S(1)}, bf16[4096,128]{1,0:T(8,128)(2,1)}, u32[]{:S(2)}) copy-start(bf16[4096,128]{1,0:T(8,128)(2,1)} %param.39) | copy-start | bytes 3145732
  182.7 24.0 %copy-start.19 = (f32[64,2]{0,1:T(2,128)S(1)}, f32[64,2]{0,1:T(2,128)}, u32[]{:S(2)}) copy-start(f32[64,2]{0,1:T(2,128)} %param.45) | copy-start | bytes 1540
  206.8 2.2 %copy-start.6 = (f32[64,4096]{1,0:T(8,128)S(1)}, f32[64,4096]{1,0:T(8,128)}, u32[]{:S(2)}) copy-start(f32[64,4096]{1,0:T(8,128)} %shard_map.202) | copy-start | bytes 3145732
  (1 other events, 0.8 us)

commit v2 on v1

--- a/solution.py
+++ b/solution.py
@@ -1,5 +1,3 @@
-import math
-
 import jax
 import jax.numpy as jnp
 from jax import lax
@@ -127,11 +125,14 @@
     )(x)
 
 
-def gather_kernel(n_tp, pieces, x_ref, out_ref, send, recv, own_sem):
+def gather_kernel(
+    n_tp, pieces, x_ref, blocks_ref, out_ref, moved_ref, send, recv, own_sem, *semaphores
+):
+    exchange = Exchange(blocks_ref, moved_ref, *semaphores)
     tp = lax.axis_index("tp")
     rows, width = x_ref.shape
     part = width // pieces
-    greet([{"tp": flip(tp, m)} for m in masks_of(n_tp)])
+    exchange.greet()
 
     def block(d, c):
         start = pl.multiple_of(flip(tp, d) * rows, rows)
@@ -159,36 +160,52 @@
                 copy.start()
                 sends.append(copy)
         if d == 0:
+            exchange.start()
             own.start()
     for copy in sends:
         copy.wait_send()
     own.wait()
-
-
-def gather_rows(x, n_tp, pieces=2):
+    exchange.finish()
+
+
+def gather_rows(x, blocks, n_tp, pieces=2):
     rows, width = x.shape
     return pl.pallas_call(
         lambda *refs: gather_kernel(n_tp, pieces, *refs),
-        out_shape=jax.ShapeDtypeStruct((n_tp * rows, width), x.dtype),
-        in_specs=[VMEM],
-        out_specs=VMEM,
+        out_shape=[
+            jax.ShapeDtypeStruct((n_tp * rows, width), x.dtype),
+            jax.ShapeDtypeStruct(blocks.shape, blocks.dtype),
+        ],
+        in_specs=[VMEM] * 2,
+        out_specs=[VMEM] * 2,
         scratch_shapes=[
             pltpu.SemaphoreType.DMA((n_tp, pieces)),
             pltpu.SemaphoreType.DMA((n_tp, pieces)),
             pltpu.SemaphoreType.DMA,
-        ],
+        ]
+        + exchange_semaphores(blocks.shape[0]),
         compiler_params=pltpu.CompilerParams(collective_id=1, has_side_effects=True),
         cost_estimate=pl.CostEstimate(flops=0, bytes_accessed=40_000_000, transcendentals=0),
-    )(x)
-
-
-def scatter_kernel(n_tp, pieces, pairs, *refs):
+    )(x, blocks)
+
+
+def scatter_kernel(n_tp, pieces, pairs, moving, *refs):
     lefts, rights = refs[:pairs], refs[pairs : 2 * pairs]
-    out_ref, sent, got, send, recv = refs[2 * pairs :]
+    refs = refs[2 * pairs :]
+    exchange = None
+    if moving:
+        blocks_ref, out_ref, moved_ref, sent, got, send, recv = refs[:7]
+        exchange = Exchange(blocks_ref, moved_ref, *refs[7:])
+    else:
+        out_ref, sent, got, send, recv = refs
     tp = lax.axis_index("tp")
     rows, width = out_ref.shape
     part = width // pieces
-    greet([{"tp": flip(tp, m)} for m in masks_of(n_tp)])
+    if moving:
+        exchange.greet()
+        exchange.start()
+    else:
+        greet([{"tp": flip(tp, m)} for m in masks_of(n_tp)])
     copies = {}
 
     def product(d, c):
@@ -233,25 +250,34 @@
         out_ref[:, pl.ds(c * part, part)] = summed(0, c, n_tp)
     for copy in copies.values():
         copy.wait_send()
-
-
-def dot_scatter(lefts, rights, n_tp, collective, pieces=4):
+    if moving:
+        exchange.finish()
+
+
+def dot_scatter(lefts, rights, n_tp, collective, blocks=None, pieces=4):
     rows, width = lefts[0].shape[0] // n_tp, rights[0].shape[1]
-    pairs = len(lefts)
+    pairs, moving = len(lefts), blocks is not None
+    shapes = [jax.ShapeDtypeStruct((rows, width), jnp.float32)]
+    operands = (*lefts, *rights)
+    scratch = [
+        pltpu.VMEM((n_tp, rows, width), jnp.bfloat16),
+        pltpu.VMEM((n_tp, rows, width), jnp.bfloat16),
+        pltpu.SemaphoreType.DMA((n_tp, pieces)),
+        pltpu.SemaphoreType.DMA((n_tp, pieces)),
+    ]
+    if moving:
+        shapes.append(jax.ShapeDtypeStruct(blocks.shape, blocks.dtype))
+        operands += (blocks,)
+        scratch += exchange_semaphores(blocks.shape[0])
     return pl.pallas_call(
-        lambda *refs: scatter_kernel(n_tp, pieces, pairs, *refs),
-        out_shape=jax.ShapeDtypeStruct((rows, width), jnp.float32),
-        in_specs=[VMEM] * (2 * pairs),
-        out_specs=VMEM,
-        scratch_shapes=[
-            pltpu.VMEM((n_tp, rows, width), jnp.bfloat16),
-            pltpu.VMEM((n_tp, rows, width), jnp.bfloat16),
-            pltpu.SemaphoreType.DMA((n_tp, pieces)),
-            pltpu.SemaphoreType.DMA((n_tp, pieces)),
-        ],
+        lambda *refs: scatter_kernel(n_tp, pieces, pairs, moving, *refs),
+        out_shape=shapes,
+        in_specs=[VMEM] * len(operands),
+        out_specs=[VMEM] * len(shapes),
+        scratch_shapes=scratch,
         compiler_params=pltpu.CompilerParams(collective_id=collective, has_side_effects=True),
         cost_estimate=pl.CostEstimate(flops=0, bytes_accessed=40_000_000, transcendentals=0),
-    )(*lefts, *rights)
+    )(*operands)
 
 
 EPS = 1e-06
@@ -259,59 +285,176 @@
 NEG_FILL = -1e30
 
 
-def rotate(values, positions):
-    half_size = values.shape[-1] // 2
-    inverse = ROPE_BASE ** (-jnp.arange(half_size, dtype=jnp.float32) * 2.0 / values.shape[-1])
-    angles = positions.astype(jnp.float32)[:, None] * inverse[None, :]
-    shaped = (angles.shape[0],) + (1,) * (values.ndim - 2) + (half_size,)
-    cosine_table = jnp.cos(angles).reshape(shaped)
-    sine_table = jnp.sin(angles).reshape(shaped)
-    first_half = values[..., :half_size]
-    second_half = values[..., half_size:]
-    return jnp.concatenate(
-        [
-            first_half * cosine_table - second_half * sine_table,
-            second_half * cosine_table + first_half * sine_table,
-        ],
-        axis=-1,
-    )
+def attend_kernel(sizes, packed, cosine, sine, *refs):
+    groups = len(sizes)
+    queries, key_ws, value_ws = refs[:groups], refs[groups : 2 * groups], refs[2 * groups : 3 * groups]
+    outs = refs[3 * groups : 4 * groups]
+    scratch = refs[4 * groups :]
+    sp = lax.axis_index("sp")
+    tok = cosine.shape[0]
+    latent_width = key_ws[0].shape[0]
+    lanes = packed.shape[1] - latent_width
+    half = ROPE // 2
+
+    def grid(shape):
+        return lax.broadcasted_iota(jnp.int32, shape, 0), lax.broadcasted_iota(jnp.int32, shape, 1)
+
+    for g, size in enumerate(sizes):
+        plain, turned, peak, total, mixed = scratch[5 * g : 5 * g + 5]
+        query = queries[g][...]
+        width = query.shape[1]
+        for h in range(plain.shape[0]):
+            i, j = grid((width, key_ws[g].shape[1]))
+            select = (i == j + h * ROPE) & (j >= h * size) & (j < (h + 1) * size)
+            plain[h] = jnp.dot(
+                query, select.astype(jnp.bfloat16), preferred_element_type=jnp.float32
+            ).astype(jnp.bfloat16)
+            i, j = grid((width, lanes))
+            base = h * (size + ROPE) + size
+            same = ((i == j + base) & (j < ROPE)).astype(jnp.float32)
+            upper = ((i == j + base + half) & (j < half)).astype(jnp.float32)
+            lower = ((i == j + base - half) & (j >= half) & (j < ROPE)).astype(jnp.float32)
+            straight = jnp.dot(
+                query, same.astype(jnp.bfloat16), preferred_element_type=jnp.float32
+            )
+            crossed = jnp.dot(
+                query, (lower - upper).astype(jnp.bfloat16), preferred_element_type=jnp.float32
+            )
+            turned[h] = (straight * cosine[...] + crossed * sine[...]).astype(jnp.bfloat16)
+        peak[...] = jnp.full_like(peak, NEG_FILL)
+        total[...] = jnp.zeros_like(total)
+        mixed[...] = jnp.zeros_like(mixed)
+
+    def one_block(index, carry):
+        start = pl.ds(pl.multiple_of(index * tok, tok), tok)
+        latent = packed[start, :latent_width]
+        turned_rows = packed[start, latent_width:]
+        i, j = grid((tok, tok))
+        visible = index * tok + j <= sp * tok + i
+        across = (((1,), (1,)), ((), ()))
+        for g, size in enumerate(sizes):
+            plain, turned, peak, total, mixed = scratch[5 * g : 5 * g + 5]
+            factor = (size + ROPE) ** (-0.5)
+            keys = jnp.dot(latent, key_ws[g][...], preferred_element_type=jnp.float32)
+            keys = keys.astype(jnp.bfloat16)
+            values = jnp.dot(latent, value_ws[g][...], preferred_element_type=jnp.float32)
+            values = values.astype(jnp.bfloat16)
+            for h in range(plain.shape[0]):
+                scores = lax.dot_general(
+                    plain[h], keys, across, preferred_element_type=jnp.float32
+                ) + lax.dot_general(
+                    turned[h], turned_rows, across, preferred_element_type=jnp.float32
+                )
+                scores = jnp.where(visible, scores * factor, NEG_FILL)
+                old = peak[h]
+                new = jnp.maximum(old, jnp.max(scores, axis=1, keepdims=True))
+                probs = jnp.where(visible, jnp.exp(scores - new), 0.0)
+                fading = jnp.exp(old - new)
+                peak[h] = new
+                total[h] = total[h] * fading + jnp.sum(probs, axis=1, keepdims=True)
+                mixed[h] = mixed[h] * fading + jnp.dot(
+                    probs.astype(jnp.bfloat16), values, preferred_element_type=jnp.float32
+                )
+        return carry
+
+    lax.fori_loop(0, sp + 1, one_block, 0)
+    for g, size in enumerate(sizes):
+        plain, turned, peak, total, mixed = scratch[5 * g : 5 * g + 5]
+        i, j = grid(outs[g].shape)
+        result = jnp.zeros(outs[g].shape, jnp.float32)
+        for h in range(plain.shape[0]):
+            own = (j >= h * size) & (j < (h + 1) * size)
+            result = jnp.where(own, mixed[h] / total[h], result)
+        outs[g][...] = result.astype(jnp.bfloat16)
+
+
+def attend(packed, cosine, sine, queries, key_ws, value_ws, sizes):
+    tok, lanes = cosine.shape
+    scratch = []
+    for g, size in enumerate(sizes):
+        heads = value_ws[g].shape[1] // size
+        scratch += [
+            pltpu.VMEM((heads, tok, key_ws[g].shape[1]), jnp.bfloat16),
+            pltpu.VMEM((heads, tok, lanes), jnp.bfloat16),
+            pltpu.VMEM((heads, tok, 1), jnp.float32),
+            pltpu.VMEM((heads, tok, 1), jnp.float32),
+            pltpu.VMEM((heads, tok, value_ws[g].shape[1]), jnp.float32),
+        ]
+    return pl.pallas_call(
+        lambda *refs: attend_kernel(sizes, *refs),
+        out_shape=[jax.ShapeDtypeStruct((tok, w.shape[1]), jnp.bfloat16) for w in value_ws],
+        in_specs=[VMEM] * (3 + 3 * len(sizes)),
+        out_specs=[VMEM] * len(sizes),
+        scratch_shapes=scratch,
+    )(packed, cosine, sine, *queries, *key_ws, *value_ws)
+
+
+class Exchange:
+    def __init__(self, source, dest, send, recv, own_sem):
+        self.refs = source, dest, send, recv
+        self.sp, self.tp = lax.axis_index("sp"), lax.axis_index("tp")
+        self.n_sp, self.n_tp = lax.axis_size("sp"), lax.axis_size("tp")
+        self.count = self.n_sp * self.n_tp
+        self.me = self.sp * self.n_tp + self.tp
+        self.own = pltpu.make_async_copy(source.at[self.me], dest.at[self.me], own_sem)
+
+    def target(self, k):
+        return (
+            lax.rem(self.sp + k // self.n_tp, self.n_sp),
+            lax.rem(self.tp + lax.rem(k, self.n_tp), self.n_tp),
+        )
+
+    def greet(self):
+        barrier = pltpu.get_barrier_semaphore()
+
+        def one(k, carry):
+            sp, tp = self.target(k)
+            pl.semaphore_signal(
+                barrier, inc=1, device_id={"sp": sp, "tp": tp}, device_id_type=MESH
+            )
+            return carry
+
+        lax.fori_loop(1, self.count, one, 0)
+        pl.semaphore_wait(barrier, self.count - 1)
+
+    def copy(self, k):
+        source, dest, send, recv = self.refs
+        sp, tp = self.target(k)
+        return remote(
+            source.at[sp * self.n_tp + tp],
+            dest.at[self.me],
+            send.at[k],
+            recv.at[k],
+            {"sp": sp, "tp": tp},
+        )
+
+    def start(self):
+        def one(k, carry):
+            self.copy(self.count - k).start()
+            return carry
+
+        lax.fori_loop(1, self.count, one, 0)
+        self.own.start()
+
+    def finish(self):
+        def one(k, carry):
+            self.copy(k).wait()
+            return carry
+
+        lax.fori_loop(1, self.count, one, 0)
+        self.own.wait()
+
+
+def exchange_semaphores(count):
+    return [
+        pltpu.SemaphoreType.DMA((count,)),
+        pltpu.SemaphoreType.DMA((count,)),
+        pltpu.SemaphoreType.DMA,
+    ]
 
 
 def rms_scale(values, gain):
     return values * lax.rsqrt(jnp.mean(values * values, axis=-1, keepdims=True) + EPS) * gain
-
-
-def update(state, query_plain, query_turned, keys, turned_rows, values, visible, factor):
-    running_max, running_sum, weighted = state
-    scores = jnp.einsum("qhd,khd->hqk", query_plain, keys, preferred_element_type=jnp.float32)
-    scores = scores + jnp.einsum(
-        "qhr,kr->hqk", query_turned, turned_rows, preferred_element_type=jnp.float32
-    )
-    scores = jnp.where(visible[None], scores * factor, NEG_FILL)
-    new_max = jnp.maximum(running_max, jnp.max(scores, axis=2))
-    probs = jnp.where(visible[None], jnp.exp(scores - new_max[:, :, None]), 0.0)
-    fading = jnp.exp(running_max - new_max)
-    running_sum = running_sum * fading + jnp.sum(probs, axis=2)
-    weighted = weighted * fading[:, :, None] + jnp.einsum(
-        "hqk,khd->hqd", probs.astype(jnp.bfloat16), values, preferred_element_type=jnp.float32
-    )
-    return (new_max, running_sum, weighted)
-
-
-def empty_state(heads, queries, value_size):
-    return (
-        jnp.full((heads, queries), NEG_FILL, jnp.float32),
-        jnp.zeros((heads, queries), jnp.float32),
-        jnp.zeros((heads, queries, value_size), jnp.float32),
-    )
-
-
-def finish(state):
-    normal_sampler = state[2] / state[1][:, :, None]
-    heads, queries, value_size = normal_sampler.shape
-    return (
-        normal_sampler.astype(jnp.bfloat16).transpose(1, 0, 2).reshape(queries, heads * value_size)
-    )
 
 
 def body(
@@ -340,101 +483,35 @@
     tok_dev = latent.shape[0]
     seq_index = lax.axis_index("sp")
     own_pos = seq_index * tok_dev + jnp.arange(tok_dev, dtype=jnp.int32)
-    last_pos = seq_index * tok_dev + tok_dev - 1
+    n_sp, n_tp = lax.axis_size("sp"), lax.axis_size("tp")
     normed_latent = rms_scale(latent.astype(jnp.float32), latent_norm_scale).astype(jnp.bfloat16)
-    turned_key = rotate(rope_key.astype(jnp.float32), own_pos).astype(jnp.bfloat16)
-    wide_heads_q = wide_query.reshape(tok_dev, -1, WIDE_HEAD_SIZE + ROPE)
-    wide_plain = wide_heads_q[..., :WIDE_HEAD_SIZE]
-    wide_turned = rotate(wide_heads_q[..., WIDE_HEAD_SIZE:].astype(jnp.float32), own_pos).astype(
-        jnp.bfloat16
-    )
-    narrow_heads_q = narrow_query.reshape(tok_dev, -1, NARROW_HEAD_SIZE + ROPE)
-    narrow_plain = narrow_heads_q[..., :NARROW_HEAD_SIZE]
-    narrow_turned = rotate(
-        narrow_heads_q[..., NARROW_HEAD_SIZE:].astype(jnp.float32), own_pos
+    half = ROPE // 2
+    lane = jnp.arange(ROPE + -ROPE % 128, dtype=jnp.int32)
+    inverse = ROPE_BASE ** (-(lane % half).astype(jnp.float32) * 2.0 / ROPE)
+    angles = own_pos.astype(jnp.float32)[:, None] * inverse[None, :]
+    cosine, sine = jnp.cos(angles), jnp.sin(angles)
+    row = jnp.arange(ROPE, dtype=jnp.int32)[:, None]
+    same = (row == lane[None, :]).astype(jnp.bfloat16)
+    cross = (row == lane[None, :] - half).astype(jnp.bfloat16) * (lane < ROPE)[None, :] - (
+        (row == lane[None, :] + half) & (lane < half)[None, :]
     ).astype(jnp.bfloat16)
-    wide_local = wide_plain.shape[1]
-    narrow_local = narrow_plain.shape[1]
-    wide_factor = (WIDE_HEAD_SIZE + ROPE) ** (-0.5)
-    narrow_factor = (NARROW_HEAD_SIZE + ROPE) ** (-0.5)
-    initial = empty_state(wide_local, tok_dev, WIDE_HEAD_SIZE) + empty_state(
-        narrow_local, tok_dev, NARROW_HEAD_SIZE
-    )
-    n_sp, n_tp = lax.axis_size("sp"), lax.axis_size("tp")
-    latent_width = latent.shape[1]
-    packed = jnp.concatenate(
-        [normed_latent, jnp.pad(turned_key, ((0, 0), (0, -turned_key.shape[1] % 128)))], axis=1
-    )
-    packed = spread(packed, n_sp, n_tp)
-    pieces = (packed[:, :latent_width], packed[:, latent_width : latent_width + ROPE])
-    indices = jnp.arange(pieces[0].shape[0], dtype=jnp.int32)
-    placing = lambda positions: positions
-    latent_rows, turned_rows = pieces
-    length_rows = latent_rows.shape[0]
-    block = math.gcd(length_rows, 512)
-
-    def one_block(block_index, inner):
-        lat_block = lax.dynamic_slice_in_dim(latent_rows, block_index * block, block, 0)
-        turned_block = lax.dynamic_slice_in_dim(turned_rows, block_index * block, block, 0)
-        key_pos = placing(lax.dynamic_slice_in_dim(indices, block_index * block, block, 0))
-
-        def work(current):
-            visible = key_pos[None, :] <= own_pos[:, None]
-            wide_keys = (
-                jnp.dot(lat_block, wide_key_weight, preferred_element_type=jnp.float32)
-                .astype(jnp.bfloat16)
-                .reshape(block, wide_local, WIDE_HEAD_SIZE)
-            )
-            wide_values = (
-                jnp.dot(lat_block, wide_value_weight, preferred_element_type=jnp.float32)
-                .astype(jnp.bfloat16)
-                .reshape(block, wide_local, WIDE_HEAD_SIZE)
-            )
-            narrow_keys = (
-                jnp.dot(lat_block, narrow_key_weight, preferred_element_type=jnp.float32)
-                .astype(jnp.bfloat16)
-                .reshape(block, narrow_local, NARROW_HEAD_SIZE)
-            )
-            narrow_values = (
-                jnp.dot(lat_block, narrow_value_weight, preferred_element_type=jnp.float32)
-                .astype(jnp.bfloat16)
-                .reshape(block, narrow_local, NARROW_HEAD_SIZE)
-            )
-            wide_state = update(
-                current[:3],
-                wide_plain,
-                wide_turned,
-                wide_keys,
-                turned_block,
-                wide_values,
-                visible,
-                wide_factor,
-            )
-            narrow_state = update(
-                current[3:],
-                narrow_plain,
-                narrow_turned,
-                narrow_keys,
-                turned_block,
-                narrow_values,
-                visible,
-                narrow_factor,
-            )
-            return wide_state + narrow_state
-
-        return lax.cond(jnp.min(key_pos) <= last_pos, work, lambda current: current, inner)
-
-    final = lax.fori_loop(0, length_rows // block, one_block, initial)
-    wide_mix = finish(final[:3])
-    narrow_mix = finish(final[3:])
-    projected = dot_scatter((wide_mix, narrow_mix), (out_wide, out_narrow), n_tp, 2)
+    turned_key = (
+        jnp.dot(rope_key, same, preferred_element_type=jnp.float32) * cosine
+        + jnp.dot(rope_key, cross.astype(jnp.bfloat16), preferred_element_type=jnp.float32) * sine
+    ).astype(jnp.bfloat16)
+    packed = spread(jnp.concatenate([normed_latent, turned_key], axis=1), n_sp, n_tp)
+    wide_mix, narrow_mix = attend(
+        packed,
+        cosine,
+        sine,
+        (wide_query, narrow_query),
+        (wide_key_weight, narrow_key_weight),
+        (wide_value_weight, narrow_value_weight),
+        (WIDE_HEAD_SIZE, NARROW_HEAD_SIZE),
+    )
+    (projected,) = dot_scatter((wide_mix, narrow_mix), (out_wide, out_narrow), n_tp, 2)
     stream = (residual.astype(jnp.float32) + projected).astype(jnp.bfloat16)
     normed = rms_scale(stream.astype(jnp.float32), ffn_gain).astype(jnp.bfloat16)
-    piece = gather_rows(normed, n_tp)
-    gate_part = jnp.dot(piece, shared_gate, preferred_element_type=jnp.float32)
-    up_part = jnp.dot(piece, shared_up, preferred_element_type=jnp.float32)
-    active = (jax.nn.silu(gate_part) * up_part).astype(jnp.bfloat16)
-    shared = dot_scatter((active,), (shared_down,), n_tp, 3)
     rows_here, top_count = routes.shape
     local_experts = expert_gate.shape[0]
     experts_all = local_experts * lax.axis_size(("sp", "tp"))
@@ -455,9 +532,11 @@
         axis=2,
     ).astype(jnp.bfloat16)
     outgoing = jnp.dot(send_map, normed, preferred_element_type=jnp.float32).astype(jnp.bfloat16)
-    outgoing = outgoing.reshape(experts_all, capacity, model_width)
-    incoming = lax.all_to_all(outgoing, ("sp", "tp"), split_axis=0, concat_axis=0, tiled=True)
-    sources = incoming.shape[0] // local_experts
+    devices = n_sp * n_tp
+    outgoing = outgoing.reshape(devices, local_experts * capacity, model_width)
+    piece, incoming = gather_rows(normed, outgoing, n_tp)
+    sources = devices
+    incoming = incoming.reshape(experts_all, capacity, model_width)
     grouped = incoming.reshape(sources, local_experts, incoming.shape[1], model_width)
     gate_part = jnp.einsum(
         "sxcd,xdf->sxcf", grouped, expert_gate, preferred_element_type=jnp.float32
@@ -467,8 +546,11 @@
     finished = jnp.einsum(
         "sxcf,xfd->sxcd", active, expert_down, preferred_element_type=jnp.float32
     ).astype(jnp.bfloat16)
-    returned = lax.all_to_all(
-        finished.reshape(incoming.shape), ("sp", "tp"), split_axis=0, concat_axis=0, tiled=True
+    gate_part = jnp.dot(piece, shared_gate, preferred_element_type=jnp.float32)
+    up_part = jnp.dot(piece, shared_up, preferred_element_type=jnp.float32)
+    active = (jax.nn.silu(gate_part) * up_part).astype(jnp.bfloat16)
+    shared, returned = dot_scatter(
+        (active,), (shared_down,), n_tp, 3, finished.reshape(outgoing.shape)
     )
     slot_rows = returned.reshape(experts_all * capacity, model_width)
     by_choice = target.reshape(rows_here, top_count)

time: 213 us -> 189 us (0.89)
  the two profiles are of different devices: /device:TPU:27 before, /device:TPU:0 now
where the time goes in v2:
time: 189 us; the launch traced here: 188 us
  Pallas kernels  160 us (85%)
  matrix products  21.1 us (11%)
  other arithmetic  5.99 us (3%)
    pallas_call x2, Pallas kernels, dot_scatter(): pl.pallas_call(lambda *refs: scatter_kernel(n_tp, pieces, pairs, moving,...  73.3 us
    pallas_call x1, Pallas kernels, gather_rows(): pl.pallas_call(lambda *refs: gather_kernel(n_tp, pieces, *refs), out_shap...  61.2 us
    pallas_call x1, Pallas kernels, spread(): pl.pallas_call(lambda *refs: spread_kernel(n_sp, n_tp, *refs), out_shape=...  20.1 us
    pallas_call x1, Pallas kernels, attend(): pl.pallas_call(lambda *refs: attend_kernel(sizes, *refs), out_shape=[jax....  5.87 us
    dot_general x1, matrix products, body(): jnp.einsum('sxcf,xfd->sxcd', active, expert_down, preferred_element_type=...  5.86 us

profile of v2, /device:TPU:0, one launch (start us, length us, event | category | flops | bytes accessed | tf_op | source)
XLA Modules:
  0.0 188.5 jit_solution(10074779783587421280)
XLA Ops:
  0.0 1.4 fusion.25
  1.4 1.3 fusion.27
  2.7 1.1 fusion.34
  3.8 1.1 fusion.36
  4.9 0.8 pad_maximum_fusion.refs_0_
  5.7 20.1 %shard_map.199.refs_0_ = bf16[1024,640]{1,0:T(8,128)(2,1)} custom-call(bf16[256,640]{1,0:T(8,128)(2,1)} %pad_maximum_fusion.refs_0_), custom_call_target="tpu_custom_call" | custom-call | bytes 30000000 | tf_op jit(solution)/shard_map/pallas_call | solution.py:111
  25.8 1.2 multiply_sine_fusion
  27.0 5.9 %shard_map.200 = (bf16[256,256]{1,0:T(8,128)(2,1)}, bf16[256,128]{1,0:T(8,128)(2,1)}) custom-call(bf16[1024,640]{1,0:T(8,128)(2,1)} %shard_map.199.refs_0_, f32[256,128]{1,0:T(8,128)} %get-tuple-element.20.refs_1_, f32[256,128]{1,0:T(8,128)} %get-tuple-element.19.refs_2_, bf16[256,384]{1,0:T(8,128)(2,1)} %refs_3_.2, bf16[256,256]{1,0:T(8,128)(2,1)} %refs_4_.1, ...), custom_call_target="tpu_custom_call" | custom-call | tf_op jit(solution)/shard_map/pallas_call | solution.py:383
  32.9 19.3 %shard_map.201 = f32[64,4096]{1,0:T(8,128)} custom-call(bf16[256,256]{1,0:T(8,128)(2,1)} %get-tuple-element.11.refs_0_, bf16[256,128]{1,0:T(8,128)(2,1)} %get-tuple-element.12.refs_1_, bf16[256,4096]{1,0:T(8,128)(2,1)} %refs_2_.1, bf16[128,4096]{1,0:T(8,128)(2,1)} %refs_3_.3), custom_call_target="tpu_custom_call" | custom-call | bytes 40000000 | tf_op jit(solution)/shard_map/pallas_call | solution.py:272
  52.2 0.0 copy-start.7
  52.3 0.0 copy-start.8
  52.3 1.5 fusion.31
  53.8 0.2 fusion.33.refs_0_
  54.0 0.0 copy-start.2
  54.0 0.1 copy.40
  54.1 0.1 eq.105
  54.3 0.2 fusion.28
  54.4 0.1 convert_element_type.93
  54.6 0.1 copy.41
  54.7 0.1 fusion.43
  54.8 2.1 %convolution_convert_fusion.1 = bf16[256,4096]{1,0:T(8,128)(2,1)} fusion(pred[256,64]{0,1:T(8,128)(4,1)S(1)} %fusion.43, bf16[64,4096]{1,0:T(8,128)(2,1)S(1)} %fusion.33.refs_0_), kind=kOutput, calls=%fused_computation.1 | convolution fusion | flops 135266304 | bytes 2637824 | tf_op jit(solution)/shard_map/dot_general | solution.py:534
  56.9 61.2 %shard_map.202 = (bf16[256,4096]{1,0:T(8,128)(2,1)}, bf16[16,16,4096]{2,1,0:T(8,128)(2,1)}) custom-call(bf16[64,4096]{1,0:T(8,128)(2,1)} %copy-done.2, bf16[16,16,4096]{2,1,0:T(8,128)(2,1)} %bitcast.82), custom_call_target="tpu_custom_call" | custom-call | bytes 40000000 | tf_op jit(solution)/shard_map/pallas_call | solution.py:173
  118.1 2.8 %fusion.8 = f32[16,1,16,192]{3,2,0,1:T(8,128)S(1)} fusion(bf16[16,16,4096]{2,1,0:T(8,128)(2,1)} %get-tuple-element.14, bf16[1,4096,192]{1,2,0:T(8,128)(2,1)} %param.37), kind=kOutput, calls=%fused_computation.15 | convolution fusion | flops 402653184 | bytes 3866624 | tf_op jit(solution)/shard_map/sxcd,xdf->sxcf/dot_general | solution.py:541
  120.9 0.0 copy-start.4
  120.9 5.9 %convolution_convert_fusion.refs_2_ = bf16[16,16,4096]{2,1,0:T(8,128)(2,1)} fusion(bf16[1,192,4096]{2,1,0:T(8,128)(2,1)S(1)} %copy-done, bf16[16,16,4096]{2,1,0:T(8,128)(2,1)} %get-tuple-element.14, bf16[1,4096,192]{1,2,0:T(8,128)(2,1)} %param.38, f32[16,1,16,192]{3,2,0,1:T(8,128)S(1)} %fusion.8), kind=kOutput, calls=%fused_computation | convolution fusion | flops 806649856 | bytes 7536640 | tf_op jit(solution)/shard_map/sxcf,xfd->sxcd/dot_general | solution.py:546
  126.7 2.5 %fusion.64 = f32[256,128]{1,0:T(8,128)S(1)} fusion(bf16[256,4096]{1,0:T(8,128)(2,1)} %get-tuple-element.13, bf16[4096,128]{1,0:T(8,128)(2,1)S(1)} %copy-done.4), kind=kOutput, calls=%fused_computation.88 | convolution fusion | flops 268435456 | bytes 3276800 | tf_op jit(solution)/shard_map/dot_general | solution.py:549
  129.2 0.0 copy-done.10
  129.2 1.3 fusion.26.refs_0_
  130.6 54.0 %shard_map.203 = (f32[64,4096]{1,0:T(8,128)}, bf16[16,16,4096]{2,1,0:T(8,128)(2,1)}) custom-call(bf16[256,128]{1,0:T(8,128)(2,1)} %fusion.26.refs_0_, bf16[128,4096]{1,0:T(8,128)(2,1)} %refs_1_.1, bf16[16,16,4096]{2,1,0:T(8,128)(2,1)} %convolution_convert_fusion.refs_2_), custom_call_target="tpu_custom_call" | custom-call | bytes 40000000 | tf_op jit(solution)/shard_map/pallas_call | solution.py:272
  184.6 2.3 %convolution_multiply_fusion.1 = f32[64,4096]{1,0:T(8,128)S(1)} fusion(bf16[256,4096]{1,0:T(8,128)(2,1)} %bitcast.83, f32[64]{0:T(128)S(1)} %get-tuple-element.24, s32[64]{0:T(128)S(1)} %get-tuple-element.22), kind=kOutput, calls=%fused_computation.4 | convolution fusion | flops 134496256 | bytes 3146240 | tf_op jit(solution)/shard_map/dot_general | solution.py:560
  186.9 0.2 copy-done.5
  187.0 1.5 fusion.2
  (26 shorter events, 0.1 us)
Async XLA Ops:
  0.0 120.9 %copy-start = (bf16[1,192,4096]{2,1,0:T(8,128)(2,1)S(1)}, bf16[1,192,4096]{2,1,0:T(8,128)(2,1)}, u32[]{:S(2)}) copy-start(bf16[1,192,4096]{2,1,0:T(8,128)(2,1)} %param.39) | copy-start | bytes 4718596
  32.9 19.3 %copy-start.6 = (bf16[64,4096]{1,0:T(8,128)(2,1)S(1)}, bf16[64,4096]{1,0:T(8,128)(2,1)}, u32[]{:S(2)}) copy-start(bf16[64,4096]{1,0:T(8,128)(2,1)} %param.32) | copy-start | bytes 1572868
  52.2 1.5 copy-start.7
  52.3 1.7 copy-start.8
  54.0 2.9 %copy-start.2 = (bf16[64,4096]{1,0:T(8,128)(2,1)}, bf16[64,4096]{1,0:T(8,128)(2,1)S(1)}, u32[]{:S(2)}) copy-start(bf16[64,4096]{1,0:T(8,128)(2,1)S(1)} %fusion.33.refs_0_) | copy-start | bytes 1572868
  120.9 5.9 %copy-start.4 = (bf16[4096,128]{1,0:T(8,128)(2,1)S(1)}, bf16[4096,128]{1,0:T(8,128)(2,1)}, u32[]{:S(2)}) copy-start(bf16[4096,128]{1,0:T(8,128)(2,1)} %param.34) | copy-start | bytes 3145732
  126.7 2.5 %copy-start.3 = (bf16[256,4096]{1,0:T(8,128)(2,1)S(1)}, bf16[256,4096]{1,0:T(8,128)(2,1)}, u32[]{:S(2)}) copy-start(bf16[256,4096]{1,0:T(8,128)(2,1)} %get-tuple-element.13) | copy-start | bytes 6291460
  126.7 2.5 %copy-start.10 = (bf16[4096,128]{1,0:T(8,128)(2,1)S(1)}, bf16[4096,128]{1,0:T(8,128)(2,1)}, u32[]{:S(2)}) copy-start(bf16[4096,128]{1,0:T(8,128)(2,1)} %param.35) | copy-start | bytes 3145732
  130.6 54.0 %copy-start.9 = (f32[64,2]{0,1:T(2,128)S(1)}, f32[64,2]{0,1:T(2,128)}, u32[]{:S(2)}) copy-start(f32[64,2]{0,1:T(2,128)} %param.41) | copy-start | bytes 1540
  184.5 2.3 %copy-start.1 = (bf16[16,16,4096]{2,1,0:T(8,128)(2,1)S(1)}, bf16[16,16,4096]{2,1,0:T(8,128)(2,1)}, u32[]{:S(2)}) copy-start(bf16[16,16,4096]{2,1,0:T(8,128)(2,1)} %get-tuple-element.16) | copy-start | bytes 6291460
  184.5 2.5 %copy-start.5 = (f32[64,4096]{1,0:T(8,128)S(1)}, f32[64,4096]{1,0:T(8,128)}, u32[]{:S(2)}) copy-start(f32[64,4096]{1,0:T(8,128)} %get-tuple-element.15) | copy-start | bytes 3145732
